TPU v7x, 32 devices: a whole 2x2x4 slice. The times are simulated.
32 devices in a mesh: ep: 4 (over y, x), tp: 8 (over z, core).
Axes of the slice: x: 2, y: 2, z: 4, core: 2. Of those that a mesh axis runs over, the one named last changes fastest.
Arguments:
- mix_tokens: bfloat16 [512, 4096], P('ep'), may hold values from -6 to 6
- mix_gain: float32 [4096], replicated, may hold values from 0.1 to 1.9
- value_weight: bfloat16 [4096, 2048], P(None, 'tp'), may hold values from -0.09375 to 0.09375
- inner_weight: bfloat16 [4096, 2048], P(None, 'tp'), may hold values from -0.09375 to 0.09375
- outer_weight: bfloat16 [4096, 2048], P(None, 'tp'), may hold values from -0.09375 to 0.09375
- conv_taps: float32 [3, 2048], P(None, 'tp'), may hold values from -3 to 3
- mix_weight: bfloat16 [2048, 4096], P('tp'), may hold values from -0.125 to 0.125
- moe_tokens: bfloat16 [512, 4096], P('ep'), may hold values from -6 to 6
- moe_gain: float32 [4096], replicated, may hold values from 0.1 to 1.9
- router_group: bfloat16 [4096, 4], replicated, may hold values from -0.09375 to 0.09375
- router_expert: bfloat16 [4096, 16], replicated, may hold values from -0.09375 to 0.09375
- expert_routes: int32 [512, 2], P('ep'), may hold values from 0 to 15, as said below
- gate_weight: bfloat16 [16, 4096, 2048], P('ep', None, 'tp'), may hold values from -0.09375 to 0.09375
- up_weight: bfloat16 [16, 4096, 2048], P('ep', None, 'tp'), may hold values from -0.09375 to 0.09375
- down_weight: bfloat16 [16, 2048, 4096], P('ep', 'tp'), may hold values from -0.5 to 0.5
Outputs:
- mixer_out: bfloat16 [512, 4096], P(('ep', 'tp'))
- expert_out: bfloat16 [512, 4096], P(('ep', 'tp'))
Inputs may be any that keep to these rules, and one draw needn't show every extreme that they name: `expert_routes`: the two experts of a row are different and lie in one group of 4 consecutive expert numbers. In each aligned block of 16 rows no expert is named more than 4 times, and in every draw some experts are named exactly 4 times in every block.
All inputs are finite; a program needn't handle non-finite values.
Results may differ from a plain program's by a relative error of at most 0.0076.
Values may be sent and summed in bfloat16 or wider, within the bound.
A program may use at most 128 MiB of HBM per device.

v0:
```python
import jax
import jax.numpy as jnp
from jax import lax
from jax.sharding import PartitionSpec as P

TAPS = 3
EXPERTS = 16
GROUPS = 4
TOPK = 2
MOE_SHARE = 16
EPG = 4
CAP = 4


def from_behind(value, axis, steps):
    count = lax.axis_size(axis)
    initial, last = (max(0, -steps), min(count, count - steps))
    return lax.ppermute(value, axis, [(source, source + steps) for source in range(initial, last)])


def rms_rows(inputs, gain_vec):
    values = inputs.astype(jnp.float32)
    inverse = lax.rsqrt(jnp.mean(values * values, axis=-1, keepdims=True) + 1e-06)
    return (values * inverse * gain_vec).astype(jnp.bfloat16)


def route_weights(normed, routes, router_group, router_expert):
    group_logit = jnp.dot(normed, router_group, preferred_element_type=jnp.float32)
    expert_logit = jnp.dot(normed, router_expert, preferred_element_type=jnp.float32)
    group_exp = jnp.exp(group_logit)
    group_id = routes[:, 0] // EPG
    group_pick = (group_id[:, None] == jnp.arange(GROUPS, dtype=jnp.int32)[None, :]).astype(
        jnp.float32
    )
    group_gate = jnp.sum(group_exp * group_pick, axis=1) / jnp.sum(group_exp, axis=1)
    expert_pick = (
        routes[:, :, None] == jnp.arange(EXPERTS, dtype=jnp.int32)[None, None, :]
    ).astype(jnp.float32)
    chosen = jnp.exp(jnp.sum(expert_logit[:, None, :] * expert_pick, axis=2))
    return group_gate[:, None] * chosen / jnp.sum(chosen, axis=1, keepdims=True)


def block_ranks(routes):
    blocks = routes.shape[0]
    entries = routes.reshape(blocks, MOE_SHARE * TOPK)
    one_hot = (entries[:, :, None] == jnp.arange(EXPERTS, dtype=jnp.int32)[None, None, :]).astype(
        jnp.int32
    )
    before = jnp.cumsum(one_hot, axis=1) - one_hot
    return jnp.sum(before * one_hot, axis=2).reshape(routes.shape)


def dispatch_rows(normed, routes):
    slot_ids = routes * CAP + block_ranks(routes)
    targets = jnp.arange(EXPERTS * CAP, dtype=jnp.int32)
    select = (slot_ids[:, None, :, :] == targets[None, :, None, None]).astype(jnp.int32)
    select = jnp.sum(select, axis=3).astype(jnp.bfloat16)
    placed = jnp.einsum("bcs,bsd->bcd", select, normed, preferred_element_type=jnp.float32)
    return placed.astype(jnp.bfloat16).reshape(normed.shape[0], EXPERTS, CAP, normed.shape[2])


def expert_hidden(arrived, gate_weight, up_weight):
    gate_proj = jnp.einsum(
        "besd,edf->besf", arrived, gate_weight, preferred_element_type=jnp.float32
    )
    up_proj = jnp.einsum("besd,edf->besf", arrived, up_weight, preferred_element_type=jnp.float32)
    return (jax.nn.silu(gate_proj) * up_proj).astype(jnp.bfloat16)


def mixer_half(
    mix_tokens, mix_gain, value_weight, inner_weight, outer_weight, conv_taps, mix_weight
):
    normed = rms_rows(mix_tokens, mix_gain)
    value_proj = jnp.dot(normed, value_weight, preferred_element_type=jnp.float32)
    inner_proj = jnp.dot(normed, inner_weight, preferred_element_type=jnp.float32)
    outer_proj = jnp.dot(normed, outer_weight, preferred_element_type=jnp.float32)
    gated_in = (inner_proj * value_proj).astype(jnp.bfloat16)
    earlier = from_behind(gated_in[gated_in.shape[0] - (TAPS - 1) :], "ep", 1)
    padded = jnp.concatenate([earlier, gated_in], axis=0).astype(jnp.float32)
    seq_rows = gated_in.shape[0]
    mixed_conv = conv_taps[0] * padded[0:seq_rows]
    for tap_index in range(1, TAPS):
        mixed_conv = mixed_conv + conv_taps[tap_index] * padded[tap_index : tap_index + seq_rows]
    conv_out = (outer_proj * mixed_conv).astype(jnp.bfloat16)
    summed = lax.psum_scatter(
        jnp.dot(conv_out, mix_weight, preferred_element_type=jnp.float32),
        "tp",
        scatter_dimension=0,
        tiled=True,
    )
    return summed.astype(jnp.bfloat16)


def local(
    mix_tokens,
    mix_gain,
    value_weight,
    inner_weight,
    outer_weight,
    conv_taps,
    mix_weight,
    moe_tokens,
    moe_gain,
    router_group,
    router_expert,
    expert_routes,
    gate_weight,
    up_weight,
    down_weight,
):
    mixer_out = mixer_half(
        mix_tokens, mix_gain, value_weight, inner_weight, outer_weight, conv_taps, mix_weight
    )
    tp_index = lax.axis_index("tp")
    model_width = moe_tokens.shape[1]
    own_routes = lax.dynamic_slice_in_dim(expert_routes, tp_index * MOE_SHARE, MOE_SHARE, 0)
    own_tokens = lax.dynamic_slice_in_dim(moe_tokens, tp_index * MOE_SHARE, MOE_SHARE, 0)
    own_normed = rms_rows(own_tokens, moe_gain)
    placed = dispatch_rows(own_normed[None], own_routes[None])[0]
    arrived = lax.all_to_all(placed, "ep", split_axis=0, concat_axis=1, tiled=True)
    hidden = expert_hidden(
        lax.all_gather(arrived[None], "tp", axis=0, tiled=True), gate_weight, up_weight
    )
    local_experts = hidden.shape[1]
    slot_count = hidden.shape[2]
    per_block = local_experts * slot_count
    partial_value = jnp.einsum(
        "besf,efd->besd", hidden, down_weight, preferred_element_type=jnp.float32
    )
    summed = lax.psum_scatter(
        partial_value.reshape(per_block * lax.axis_size("tp"), model_width),
        "tp",
        scatter_dimension=0,
        tiled=True,
    )
    results = summed.astype(jnp.bfloat16).reshape(
        local_experts, slot_count // CAP, CAP, model_width
    )
    returned = lax.all_to_all(results, "ep", split_axis=1, concat_axis=0, tiled=True).reshape(
        EXPERTS * CAP, model_width
    )
    weights = route_weights(own_normed, own_routes, router_group, router_expert)
    own_slots = own_routes * CAP + block_ranks(own_routes[None])[0]
    picked = jnp.take(returned, own_slots, axis=0).astype(jnp.float32)
    expert_out = jnp.sum(weights[:, :, None] * picked, axis=1).astype(jnp.bfloat16)
    return (mixer_out, expert_out)


def solution(mesh):
    return jax.shard_map(
        local,
        mesh=mesh,
        in_specs=(
            P("ep", None),
            P(),
            P(None, "tp"),
            P(None, "tp"),
            P(None, "tp"),
            P(None, "tp"),
            P("tp", None),
            P("ep", None),
            P(),
            P(),
            P(),
            P("ep", None),
            P("ep", None, "tp"),
            P("ep", None, "tp"),
            P("ep", "tp", None),
        ),
        out_specs=(P(("ep", "tp"), None), P(("ep", "tp"), None)),
        check_vma=False,
    )
```

profile of v0, /device:TPU:0, one launch (start us, length us, event | category | flops | bytes accessed | tf_op | source)
XLA Modules:
  0.0 235.8 jit_solution(12911871643067953281)
XLA Ops:
  7.2 0.9 constant_dynamic-slice_fusion
  8.8 0.8 compare_and_fusion
  9.6 1.0 fusion.34
  10.7 1.3 convolution_convert_fusion
  12.2 13.5 %all_to_all.30 = bf16[16,4,4096]{2,1,0:T(4,128)(2,1)S(1)} all-to-all(bf16[16,4,4096]{2,1,0:T(4,128)(2,1)S(1)} %squeeze_reshape.7), channel_id=1, replica_groups=mesh['ep'=4,'tp'=8] {'ep'}, dimensions={0} | all-to-all | bytes 1048576 | tf_op jit(solution)/shard_map/all_to_all | solution.py:120
  25.9 0.9 broadcast_in_dim.12
  26.9 46.7 %all-gather.2.cloned.1.call-done = bf16[8,4,16,4096]{3,2,0,1:T(8,128)(2,1)} async-done(((bf16[1,4,16,4096]{3,2,0,1:T(8,128)(2,1)}), bf16[8,4,16,4096]{3,2,0,1:T(8,128)(2,1)}) %all-gather.2.cloned.1.call-update) | async-done | bytes 4194320 | tf_op jit(solution)/shard_map/all_gather | solution.py:122
  73.6 5.9 %fusion.12 = f32[8,4,16,256]{3,2,0,1:T(8,128)S(1)} fusion(bf16[8,4,16,4096]{3,2,0,1:T(8,128)(2,1)} %all-gather.2.cloned.1.call-done, bf16[4,4096,256]{2,1,0:T(8,128)(2,1)} %param.27), kind=kOutput, calls=%fused_computation.14 | convolution fusion | flops 1073741824 | bytes 13107200 | tf_op jit(solution)/shard_map/besd,edf->besf/dot_general | solution.py:63
  79.5 12.6 %fusion.6 = f32[8,4,16,4096]{3,2,0,1:T(8,128)} fusion(bf16[4,256,4096]{2,1,0:T(8,128)(2,1)} %param.29, bf16[8,4,16,4096]{3,2,0,1:T(8,128)(2,1)} %all-gather.2.cloned.1.call-done, bf16[4,4096,256]{2,1,0:T(8,128)(2,1)} %param.28, f32[8,4,16,256]{3,2,0,1:T(8,128)S(1)} %fusion.12), kind=kOutput, calls=%fused_computation.7 | convolution fusion | flops 2148270080 | bytes 29884416 | tf_op jit(solution)/shard_map/besf,efd->besd/dot_general | solution.py:127
  92.1 7.6 %copy.39 = f32[8,4,16,4096]{3,2,1,0:T(8,128)} copy(f32[8,4,16,4096]{3,2,0,1:T(8,128)} %fusion.6) | data formatting | bytes 16777216 | tf_op jit(solution)/shard_map/besf,efd->besd/transpose | solution.py:127
  99.8 1.1 copy-done.1
  101.2 2.2 fusion.54
  104.0 3.4 %collective-permute-start = (bf16[2,256]{1,0:T(2,128)(2,1)S(1)}, bf16[2,256]{1,0:T(2,128)(2,1)S(1)}, u32[]{:S(2)}, u32[]{:S(2)}) collective-permute-start(bf16[2,256]{1,0:T(2,128)(2,1)S(1)} %slice.34), channel_id=1, source_target_pairs={{0,8},{8,16},{16,24},{1,9},{9,17},{17,25},{2,10},{10,18},{18,26},{... | collective-permute-start | bytes 3080 | tf_op jit(solution)/shard_map/ppermute | solution.py:18
  107.4 1.3 collective-permute-done
  108.7 4.3 %fusion.28 = f32[128,4096]{1,0:T(8,128)} fusion(bf16[256,4096]{1,0:T(8,128)(2,1)S(1)} %copy-done, bf16[4096,256]{1,0:T(8,128)(2,1)} %param.19, f32[130,256]{1,0:T(8,128)S(1)} %maximum_convert_fusion, f32[256]{0:T(256)S(1)} %bitcast.67, f32[256]{0:T(256)S(1)} %bitcast.68, f32[256]{0:T(256)S(1)} %bitcast.66, bf16[128,4096]{1,0:T(8,128)(2,1)S(1)} %copy-done.1, ...), kind=kOutput, calls=%fused_computation.22 | convolution fusion | flops 539197440 | bytes 7753216 | tf_op jit(solution)/shard_map/dot_general | solution.py:86
  113.8 1.1 fusion.58
  115.0 1.1 fusion.50
  116.3 71.9 %reduce-scatter.5.cloned.1.call-done = f32[64,4096]{1,0:T(8,128)} async-done(((f32[512,4096]{1,0:T(8,128)}), f32[64,4096]{1,0:T(8,128)}) %reduce-scatter.5.cloned.1.call-update) | async-done | bytes 1048592 | tf_op jit(solution)/shard_map/reduce_scatter | solution.py:130
  188.2 1.3 convert_element_type.92
  189.7 1.0 copy.40
  190.7 3.6 %all-to-all-start.1 = ((bf16[4,4,4,4096]{3,2,0,1:T(4,128)(2,1)}), bf16[4,4,4,4096]{3,2,0,1:T(4,128)(2,1)S(1)}, u32[]{:S(2)}, u32[]{:S(2)}) async-start(bf16[4,4,4,4096]{3,2,0,1:T(4,128)(2,1)} %copy.40), calls=%async_computation.3 | async-start | bytes 1048576 | tf_op jit(solution)/shard_map/all_to_all | solution.py:139
  194.6 30.6 %reduce-scatter.3.cloned.1.call-done = f32[16,4096]{1,0:T(8,128)} async-done(((f32[128,4096]{1,0:T(8,128)}), f32[16,4096]{1,0:T(8,128)}) %reduce-scatter.3.cloned.1.call-update) | async-done | bytes 262160 | tf_op jit(solution)/shard_map/reduce_scatter | solution.py:85
  225.1 1.6 convert_element_type.84
  227.8 1.5 multiply_reduce_fusion
  (54 shorter events, 4.5 us)
Async XLA Ops:
  7.2 101.5 %copy-start = (bf16[256,4096]{1,0:T(8,128)(2,1)S(1)}, bf16[256,4096]{1,0:T(8,128)(2,1)}, u32[]{:S(2)}) copy-start(bf16[256,4096]{1,0:T(8,128)(2,1)} %param.21) | copy-start | bytes 6291460
  7.2 66.4 %all-gather.2.cloned.1.call-start = ((), (), s32[]{:S(2)}) async-start(), calls=%async_computation.5 | async-start | bytes 4718592 | tf_op jit(solution)/shard_map/all_gather | solution.py:122
  26.8 161.4 %reduce-scatter.5.cloned.1.call-start = ((), (), s32[]{:S(2)}) async-start(), calls=%async_computation.6 | async-start | bytes 9437184 | tf_op jit(solution)/shard_map/reduce_scatter | solution.py:130
  99.7 1.2 copy-start.1
  99.7 1.5 copy-start.2
  99.7 125.4 %reduce-scatter.3.cloned.1.call-start = ((), (), s32[]{:S(2)}) async-start(), calls=%async_computation.4 | async-start | bytes 2359296 | tf_op jit(solution)/shard_map/reduce_scatter | solution.py:85
  101.2 2.3 copy-start.5
  103.5 3.9 %copy-start.4 = (f32[3,256]{1,0:T(4,128)S(1)}, f32[3,256]{1,0:T(4,128)}, u32[]{:S(2)}) copy-start(f32[3,256]{1,0:T(4,128)} %param.20) | copy-start | bytes 9220
  104.0 4.7 %collective-permute-start = (bf16[2,256]{1,0:T(2,128)(2,1)S(1)}, bf16[2,256]{1,0:T(2,128)(2,1)S(1)}, u32[]{:S(2)}, u32[]{:S(2)}) collective-permute-start(bf16[2,256]{1,0:T(2,128)(2,1)S(1)} %slice.34), channel_id=1, source_target_pairs={{0,8},{8,16},{16,24},{1,9},{9,17},{17,25},{2,10},{10,18},{18,26},{... | collective-permute-start | bytes 3080 | tf_op jit(solution)/shard_map/ppermute | solution.py:18
  113.0 0.7 copy-start.3
  113.0 0.8 copy-start.7
  113.0 1.9 copy-start.6
  190.7 36.1 %all-to-all-start.1 = ((bf16[4,4,4,4096]{3,2,0,1:T(4,128)(2,1)}), bf16[4,4,4,4096]{3,2,0,1:T(4,128)(2,1)S(1)}, u32[]{:S(2)}, u32[]{:S(2)}) async-start(bf16[4,4,4,4096]{3,2,0,1:T(4,128)(2,1)} %copy.40), calls=%async_computation.3 | async-start | bytes 1048576 | tf_op jit(solution)/shard_map/all_to_all | solution.py:139
Sparse Core Ops, SparseCore 0:
  26.9 46.5 all-gather.1
  99.8 88.3 reduce-scatter.4
  190.5 34.5 reduce-scatter.2
where the time goes:
time: 236 us
  waiting for transfers between devices  150 us (64%)
  matrix products  29.2 us (12%)
  local copies, waits for them, and re-layouts  14.4 us (6%)
  between operations  14 us (6%)
  blocking collectives  13.5 us (6%)
  starting transfers between devices  7.14 us (3%)
  other arithmetic  7.12 us (3%)
    reduce_scatter x1, waiting for transfers between devices, local(): lax.psum_scatter(partial_value.reshape(per_block * lax.axis_size('tp'), m...  71.9 us
    all_gather x1, waiting for transfers between devices, local(): lax.all_gather(arrived[None], 'tp', axis=0, tiled=True)  46.7 us
    reduce_scatter x1, waiting for transfers between devices, mixer_half(): lax.psum_scatter(jnp.dot(conv_out, mix_weight, preferred_element_type=jnp...  30.6 us
    all_to_all x1, blocking collectives, local(): lax.all_to_all(placed, 'ep', split_axis=0, concat_axis=1, tiled=True)  13.5 us
    dot_general x1, matrix products, local(): jnp.einsum('besf,efd->besd', hidden, down_weight, preferred_element_type=...  12.6 us
    transpose x1, local copies, waits for them, and re-layouts, local(): jnp.einsum('besf,efd->besd', hidden, down_weight, preferred_element_type=...  7.6 us
    dot_general x1, matrix products, expert_hidden(): jnp.einsum('besd,edf->besf', arrived, gate_weight, preferred_element_type...  5.91 us
  transfers between devices with their start and end apart: 5, of which 4 were waited for; matrix products, arithmetic and copies ran while one was open for 6% of the time, Pallas kernels for 0%

commit v1 on v0

v1 whole, which is shorter than its diff:
```python
import functools

import jax
import jax.numpy as jnp
from jax import lax
from jax.experimental import pallas as pl
from jax.experimental.pallas import tpu as pltpu
from jax.sharding import PartitionSpec as P

EPG = 4
CAP = 4
CORES = 2
CHUNKS = 4
MESH = pl.DeviceIdType.MESH
F32, BF16 = jnp.float32, jnp.bfloat16


def iota(shape, dim):
    return lax.broadcasted_iota(jnp.int32, shape, dim)


def norm_rows(src, gain, dst):
    width = src.shape[1]

    def body(i, carry):
        rows = pl.ds(pl.multiple_of(i * 16, 16), 16)
        x = src[rows, :].astype(F32)
        inv = lax.rsqrt(jnp.sum(x * x, axis=1, keepdims=True) * (1.0 / width) + 1e-06)
        dst[rows, :] = (x * inv * gain[...]).astype(BF16)
        return carry

    lax.fori_loop(0, src.shape[0] // 16, body, 0)


def column_tiles(width, tile, body):
    def step(i, carry):
        body(pl.ds(pl.multiple_of(i * tile, tile), tile))
        return carry

    lax.fori_loop(0, width // tile, step, 0)


def kernel(
    cfg,
    mix_tokens, mix_gain, value_w, inner_w, outer_w, taps, mix_w, moe_tokens, moe_gain,
    router_group, router_expert, routes, gate_w, up_w, down_w,
    mixer_out, expert_out,
    xm, xe, rg, rx, vw, iw, ow, mw, gw, uw, dw,
    nm, ne, spread, pack, got, wpack, wgot, wrow,
    gated, halo, padded, conv, pair_out, pair_in, keep, zin,
    hid, y_out, y_in, y_keep, e_in, s_keep, s_out, s_in,
    load_sem, gate_sem, up_sem, down_sem,
    disp_s, disp_r, w_s, w_r, fwd_s, fwd_r, halo_s, halo_r, mp_s, mp_r, mz_s, mz_r,
    yp_s, yp_r, ye_s, ye_r, yz_s, yz_r,
):
    ep, tp, zs, half, experts_here = cfg
    e_me, t_me = lax.axis_index("ep"), lax.axis_index("tp")
    z_me, c_me = t_me // CORES, lax.rem(t_me, CORES)
    c_no = 1 - c_me
    partner = z_me * CORES + c_no
    width = xm.shape[1]
    ep_peers = [lax.rem(e_me + d, ep) for d in range(1, ep)]
    z_peers = [lax.rem(z_me + d, zs) for d in range(1, zs)]

    barrier = pltpu.get_barrier_semaphore()
    for e in ep_peers:
        pl.semaphore_signal(barrier, inc=1, device_id={"ep": e, "tp": t_me}, device_id_type=MESH)
    for z in z_peers:
        pl.semaphore_signal(
            barrier, inc=1, device_id={"ep": e_me, "tp": z * CORES + c_me}, device_id_type=MESH
        )
    pl.semaphore_signal(barrier, inc=1, device_id={"ep": e_me, "tp": partner}, device_id_type=MESH)

    def load(k, src, dst):
        return pltpu.make_async_copy(src, dst, load_sem.at[k])

    loads = [
        load(k, s, d)
        for k, (s, d) in enumerate(
            [
                (moe_tokens, xe), (router_group, rg), (router_expert, rx), (mix_tokens, xm),
                (value_w, vw), (inner_w, iw), (outer_w, ow), (mix_w, mw),
            ]
        )
    ]
    for c in loads:
        c.start()

    def remote(src, dst, s_sem, r_sem, e, t):
        return pltpu.make_async_remote_copy(
            src_ref=src, dst_ref=dst, send_sem=s_sem, recv_sem=r_sem,
            device_id={"ep": e, "tp": t}, device_id_type=MESH,
        )

    loads[0].wait()
    norm_rows(xe, moe_gain, ne)
    count = xe.shape[0]
    share = count // tp
    slots = half // zs
    span = ep * half
    r = routes[...]
    picks = [r[:, 0:1], r[:, 1:2]]
    lane = iota((count, 128), 1)
    shards = [
        sum((p >= s * experts_here).astype(jnp.int32) for s in range(1, ep)) for p in picks
    ]
    member = jnp.where((lane == shards[0]) | (lane == shards[1]), 1.0, 0.0).astype(BF16)
    ti, tj = iota((count, count), 0), iota((count, count), 1)
    earlier = jnp.where(((ti ^ tj) < share) & (tj < ti), 1.0, 0.0).astype(BF16)
    rank = jnp.dot(earlier, member, preferred_element_type=F32)
    block = lax.shift_right_logical(iota((count, 1), 0), share.bit_length() - 1)
    base = (block & 1) * span + lax.shift_right_logical(block, 1) * slots
    slot_lane = iota((count, 2 * span), 1)
    hits = []
    for s in shards:
        mine = jnp.sum(jnp.where(lane == s, rank, 0.0), axis=1, keepdims=True).astype(jnp.int32)
        hits.append(slot_lane == base + s * half + mine)
    one_hot = jnp.where(hits[0] | hits[1], 1.0, 0.0).astype(BF16)
    spread[...] = one_hot

    def pack_tile(cols):
        pack[:, cols] = lax.dot_general(
            spread[...], ne[:, cols], (((0,), (0,)), ((), ())), preferred_element_type=F32
        ).astype(BF16)

    column_tiles(width, 512, pack_tile)

    pl.semaphore_wait(barrier, (ep - 1) + (zs - 1) + 1)
    sends = []

    def go(copy):
        copy.start()
        sends.append(copy)

    def half_rows(c, e):
        return pl.ds(pl.multiple_of(c * span + e * half, half), half)

    for e in ep_peers:
        go(
            remote(
                pack.at[half_rows(c_me, e), :], got.at[half_rows(c_me, e_me), :],
                disp_s.at[e], disp_r.at[e_me], e, t_me,
            )
        )
    for k in range(experts_here):
        pltpu.make_async_copy(gate_w.at[k], gw.at[k], gate_sem.at[k]).start()
        pltpu.make_async_copy(up_w.at[k], uw.at[k], up_sem.at[k]).start()
    for k in range(experts_here):
        pltpu.make_async_copy(down_w.at[k], dw.at[k], down_sem.at[k]).start()

    loads[1].wait()
    loads[2].wait()
    group_exp = jnp.exp(jnp.dot(ne[...], rg[...], preferred_element_type=F32))
    expert_logit = jnp.dot(ne[...], rx[...], preferred_element_type=F32)
    groups, experts = group_exp.shape[1], expert_logit.shape[1]
    group = sum((picks[0] >= s * EPG).astype(jnp.int32) for s in range(1, groups))
    chosen_group = jnp.where(iota((count, groups), 1) == group, group_exp, 0.0)
    group_gate = jnp.sum(chosen_group, axis=1, keepdims=True) / jnp.sum(
        group_exp, axis=1, keepdims=True
    )
    expert_lane = iota((count, experts), 1)
    chosen = [
        jnp.exp(jnp.sum(jnp.where(expert_lane == p, expert_logit, 0.0), axis=1, keepdims=True))
        for p in picks
    ]
    scale = chosen[0] + chosen[1]
    weights = sum(
        jnp.where(lane == p, group_gate * c / scale, 0.0) for p, c in zip(picks, chosen)
    )
    parts, rest = [], weights
    for _ in range(3):
        parts.append(rest.astype(BF16))
        rest = rest - parts[-1].astype(F32)
    packed_w = sum(
        lax.dot_general(spread[...], p, (((0,), (0,)), ((), ())), preferred_element_type=F32)
        for p in parts
    )
    for e in range(ep):
        for c in range(CORES):
            wpack[e, c * half : (c + 1) * half, :] = packed_w[
                c * span + e * half : c * span + (e + 1) * half, :
            ]
    for e in ep_peers:
        go(remote(wpack.at[e], wgot.at[e_me], w_s.at[e], w_r.at[e_me], e, t_me))
    wgot[e_me] = wpack[e_me]
    for c in range(CORES):
        got[half_rows(c, e_me), :] = pack[half_rows(c, e_me), :]

    loads[3].wait()
    norm_rows(xm, mix_gain, nm)
    loads[4].wait()
    loads[5].wait()
    rows = xm.shape[0]
    value_proj = jnp.dot(nm[...], vw[...], preferred_element_type=F32)
    inner_proj = jnp.dot(nm[...], iw[...], preferred_element_type=F32)
    gated[...] = (inner_proj * value_proj).astype(BF16)
    halo_copy = remote(
        gated.at[pl.ds(rows - 16, 16), :], halo, halo_s.at[0], halo_r.at[0],
        lax.rem(e_me + 1, ep), t_me,
    )
    halo_copy.start()
    padded[8:, :] = gated[...].astype(F32)
    loads[6].wait()
    outer_proj = jnp.dot(nm[...], ow[...], preferred_element_type=F32)
    halo_copy.wait()
    before = halo[...].astype(F32)[8:16, :]
    padded[0:8, :] = jnp.where(e_me > 0, before, jnp.zeros_like(before))
    n_taps = taps.shape[0]
    mixed = taps[0:1, :] * padded[pl.ds(9 - n_taps, rows), :]
    for j in range(1, n_taps):
        mixed = mixed + taps[j : j + 1, :] * padded[pl.ds(9 - n_taps + j, rows), :]
    conv[...] = (outer_proj * mixed).astype(BF16)
    mix_share = rows // tp

    def parity_rows(ref, c, step, cols):
        return jnp.concatenate(
            [
                ref[pl.ds(pl.multiple_of((z * CORES + c) * step, step), step), cols]
                for z in range(zs)
            ],
            axis=0,
        )

    loads[7].wait()
    everything = slice(None)

    def partner_tile(cols):
        pair_out[:, cols] = jnp.dot(
            parity_rows(conv, c_no, mix_share, everything), mw[:, cols], preferred_element_type=F32
        ).astype(BF16)

    column_tiles(width, 512, partner_tile)
    pair_copy = remote(pair_out, pair_in, mp_s.at[0], mp_r.at[0], e_me, partner)
    go(pair_copy)

    def own_tile(cols):
        keep[:, cols] = jnp.dot(
            parity_rows(conv, c_me, mix_share, everything), mw[:, cols], preferred_element_type=F32
        )

    column_tiles(width, 512, own_tile)
    pair_copy.wait_recv()

    def sum_tile(cols):
        total = keep[:, cols] + pair_in[:, cols].astype(F32)
        keep[:, cols] = total
        pair_in[:, cols] = total.astype(BF16)

    column_tiles(width, 512, sum_tile)

    def z_rows(z, step):
        return pl.ds(pl.multiple_of(z * step, step), step)

    for z in z_peers:
        go(
            remote(
                pair_in.at[z_rows(z, mix_share), :], zin.at[z_me], mz_s.at[z], mz_r.at[z_me],
                e_me, z * CORES + c_me,
            )
        )

    for e in ep_peers:
        here = got.at[half_rows(c_me, e), :]
        remote(here, here, disp_s.at[e], disp_r.at[e], e, t_me).wait_recv()
        go(remote(here, here, fwd_s.at[e], fwd_r.at[e], e_me, partner))
    for e in ep_peers:
        remote(wgot.at[e], wgot.at[e], w_s.at[e], w_r.at[e], e, t_me).wait_recv()
    for c in range(CORES):
        for e in range(ep):
            wrow[c * span + e * half : c * span + (e + 1) * half, :] = wgot[
                e, c * half : (c + 1) * half, :
            ]
    for e in ep_peers:
        there = got.at[half_rows(c_no, e), :]
        remote(there, there, fwd_s.at[e], fwd_r.at[e], e_me, partner).wait_recv()

    hidden = gw.shape[2]
    arrived_lane = iota((2 * span, 128), 1)
    for k in range(experts_here):
        pltpu.make_async_copy(gate_w.at[k], gw.at[k], gate_sem.at[k]).wait()
        pltpu.make_async_copy(up_w.at[k], uw.at[k], up_sem.at[k]).wait()

    def expert(k, carry):
        gate = jnp.dot(got[...], gw[k], preferred_element_type=F32)
        up = jnp.dot(got[...], uw[k], preferred_element_type=F32)
        weight = jnp.sum(
            jnp.where(arrived_lane == e_me * experts_here + k, wrow[...], 0.0),
            axis=1, keepdims=True,
        )
        value = gate / (1.0 + jnp.exp(-gate)) * up * weight
        hid[k] = value.astype(BF16)
        return carry

    lax.fori_loop(0, experts_here, expert, 0)
    for k in range(experts_here):
        pltpu.make_async_copy(down_w.at[k], dw.at[k], down_sem.at[k]).wait()

    chunk = width // CHUNKS
    tile = min(512, chunk)

    def core_rows(c):
        return pl.ds(pl.multiple_of(c * span, span), span)

    def down(c, cols):
        total = jnp.dot(hid[0, core_rows(c), :], dw[0, :, cols], preferred_element_type=F32)
        for k in range(1, experts_here):
            total = total + jnp.dot(
                hid[k, core_rows(c), :], dw[k, :, cols], preferred_element_type=F32
            )
        return total

    y_copies = {}

    def stage_a(j):
        for i in range(chunk // tile):
            at = slice(i * tile, (i + 1) * tile)
            cols = slice(j * chunk + i * tile, j * chunk + (i + 1) * tile)
            y_out[j, :, at] = down(c_no, cols).astype(BF16)
        y_copies[j] = remote(y_out.at[j], y_in.at[j], yp_s.at[j], yp_r.at[j], e_me, partner)
        go(y_copies[j])
        for i in range(chunk // tile):
            at = slice(i * tile, (i + 1) * tile)
            cols = slice(j * chunk + i * tile, j * chunk + (i + 1) * tile)
            y_keep[j % 2, :, at] = down(c_me, cols)

    def e_rows(e):
        return pl.ds(pl.multiple_of(e * half, half), half)

    def stage_b(j):
        y_copies[j].wait_recv()
        y_in[j] = (y_keep[j % 2] + y_in[j].astype(F32)).astype(BF16)
        for e in ep_peers:
            go(
                remote(
                    y_in.at[j, e_rows(e), :], e_in.at[j, e_rows(e_me), :],
                    ye_s.at[j, e], ye_r.at[j, e_me], e, t_me,
                )
            )
        e_in[j, e_rows(e_me), :] = y_in[j, e_rows(e_me), :]

    def stage_c(j):
        for e in ep_peers:
            here = e_in.at[j, e_rows(e), :]
            remote(here, here, ye_s.at[j, e], ye_r.at[j, e], e, t_me).wait_recv()
        own = parity_rows(spread, c_me, share, core_rows(c_me))
        total = jnp.dot(own, e_in[j], preferred_element_type=F32)
        s_out[j] = total.astype(BF16)
        for z in z_peers:
            go(
                remote(
                    s_out.at[j, z_rows(z, share), :], s_in.at[j, z_me],
                    yz_s.at[j, z], yz_r.at[j, z_me], e_me, z * CORES + c_me,
                )
            )
        s_keep[j % 2] = total

    def stage_d(j):
        total = s_keep[j % 2, z_rows(z_me, share), :]
        for z in z_peers:
            here = s_in.at[j, z]
            remote(here, here, yz_s.at[j, z], yz_r.at[j, z], e_me, z * CORES + c_me).wait_recv()
            total = total + s_in[j, z].astype(F32)
        expert_out[:, j * chunk : (j + 1) * chunk] = total.astype(BF16)

    for j in range(CHUNKS):
        stage_a(j)
        if j:
            stage_b(j - 1)
    stage_b(CHUNKS - 1)

    total = keep[z_rows(z_me, mix_share), :]
    for z in z_peers:
        here = zin.at[z]
        remote(here, here, mz_s.at[z], mz_r.at[z], e_me, z * CORES + c_me).wait_recv()
        total = total + zin[z].astype(F32)
    mixer_out[...] = total.astype(BF16)

    for j in range(CHUNKS):
        stage_c(j)
        if j:
            stage_d(j - 1)
    stage_d(CHUNKS - 1)
    for copy in sends:
        copy.wait_send()


def local(ep, tp, *args):
    (mix_tokens, mix_gain, value_w, inner_w, outer_w, taps, mix_w, moe_tokens, moe_gain,
     router_group, router_expert, routes, gate_w, up_w, down_w) = args
    rows, width = mix_tokens.shape
    count = moe_tokens.shape[0]
    channels, hidden = value_w.shape[1], gate_w.shape[2]
    experts_here = gate_w.shape[0]
    zs = tp // CORES
    share, mix_share = count // tp, rows // tp
    topk = routes.shape[1]
    slots = experts_here * CAP
    if experts_here % EPG == 0:
        slots = slots // topk
    slots = min(slots, share)
    half = zs * slots
    span = ep * half
    chunk = width // CHUNKS
    any_ref = pl.BlockSpec(memory_space=pl.ANY)
    vmem = pl.BlockSpec(memory_space=pltpu.VMEM)
    V, D = pltpu.VMEM, lambda *s: pltpu.SemaphoreType.DMA(s)
    scratch = [
        V((rows, width), BF16), V((count, width), BF16),
        V(router_group.shape, BF16), V(router_expert.shape, BF16),
        V(value_w.shape, BF16), V(inner_w.shape, BF16), V(outer_w.shape, BF16),
        V(mix_w.shape, BF16),
        V(gate_w.shape, BF16), V(up_w.shape, BF16), V(down_w.shape, BF16),
        V((rows, width), BF16), V((count, width), BF16), V((count, 2 * span), BF16),
        V((2 * span, width), BF16), V((2 * span, width), BF16),
        V((ep, 2 * half, 128), F32), V((ep, 2 * half, 128), F32), V((2 * span, 128), F32),
        V((rows, channels), BF16), V((16, channels), BF16), V((rows + 8, channels), F32),
        V((rows, channels), BF16),
        V((zs * mix_share, width), BF16), V((zs * mix_share, width), BF16),
        V((zs * mix_share, width), F32),
        V((zs, mix_share, width), BF16),
        V((experts_here, 2 * span, hidden), BF16),
        V((CHUNKS, span, chunk), BF16), V((CHUNKS, span, chunk), BF16),
        V((2, span, chunk), F32),
        V((CHUNKS, span, chunk), BF16),
        V((2, zs * share, chunk), F32), V((CHUNKS, zs * share, chunk), BF16),
        V((CHUNKS, zs, share, chunk), BF16),
        D(8), D(experts_here), D(experts_here), D(experts_here),
        D(ep), D(ep), D(ep), D(ep), D(ep), D(ep), D(1), D(1), D(1), D(1), D(zs), D(zs),
        D(CHUNKS), D(CHUNKS), D(CHUNKS, ep), D(CHUNKS, ep), D(CHUNKS, zs), D(CHUNKS, zs),
    ]
    out = [
        jax.ShapeDtypeStruct((mix_share, width), BF16),
        jax.ShapeDtypeStruct((share, width), BF16),
    ]
    in_specs = [
        any_ref, vmem, any_ref, any_ref, any_ref, vmem, any_ref, any_ref, vmem,
        any_ref, any_ref, vmem, any_ref, any_ref, any_ref,
    ]
    return pl.pallas_call(
        functools.partial(kernel, (ep, tp, zs, half, experts_here)),
        out_shape=out,
        in_specs=in_specs,
        out_specs=[vmem, vmem],
        scratch_shapes=scratch,
        compiler_params=pltpu.CompilerParams(
            collective_id=0, has_side_effects=True, vmem_limit_bytes=67043328
        ),
        name="mixer_and_experts",
    )(
        mix_tokens, mix_gain.reshape(1, width), value_w, inner_w, outer_w, taps, mix_w,
        moe_tokens, moe_gain.reshape(1, width), router_group, router_expert, routes,
        gate_w, up_w, down_w,
    )


def solution(mesh):
    return jax.shard_map(
        lambda *args: tuple(local(mesh.shape["ep"], mesh.shape["tp"], *args)),
        mesh=mesh,
        in_specs=(
            P("ep", None), P(), P(None, "tp"), P(None, "tp"), P(None, "tp"), P(None, "tp"),
            P("tp", None), P("ep", None), P(), P(), P(), P("ep", None),
            P("ep", None, "tp"), P("ep", None, "tp"), P("ep", "tp", None),
        ),
        out_specs=(P(("ep", "tp"), None), P(("ep", "tp"), None)),
        check_vma=False,
    )
```

time: 236 us -> 66.7 us (0.28)
  waiting for transfers between devices: 150 us -> 0 us
  Pallas kernels: 0 us -> 56.8 us
  matrix products: 29.2 us -> 0 us
  blocking collectives: 13.5 us -> 0 us
  between operations: 14 us -> 0.64 us
  starting transfers between devices: 7.14 us -> 0 us
  other arithmetic: 7.12 us -> 0 us
  local copies, waits for them, and re-layouts: 14.4 us -> 8.99 us
    reduce_scatter x2 -> x0, waiting for transfers between devices: 102 us -> none  [the longest x1 71.9 us: local(): lax.psum_scatter(partial_value.reshape(per_block * lax.axis_size('tp'), m...]
    pallas_call x0 -> x1, Pallas kernels: none -> 56.8 us  [local(): pl.pallas_call(functools.partial(kernel, (ep, tp, zs, half, experts_here)...]
    all_gather x1 -> x0, waiting for transfers between devices: 46.7 us -> none  [local(): lax.all_gather(arrived[None], 'tp', axis=0, tiled=True)]
    dot_general x8 -> x0, matrix products: 29.2 us -> none  [the longest x1 12.6 us: local(): jnp.einsum('besf,efd->besd', hidden, down_weight, preferred_element_type=...]
    all_to_all x1 -> x0, blocking collectives: 13.5 us -> none  [local(): lax.all_to_all(placed, 'ep', split_axis=0, concat_axis=1, tiled=True)]
    transpose x1 -> x0, local copies, waits for them, and re-layouts: 7.6 us -> none  [local(): jnp.einsum('besf,efd->besd', hidden, down_weight, preferred_element_type=...]
    unnamed x16 -> x5, local copies, waits for them, and re-layouts: 1.72 us -> 8.99 us
    all_to_all x1 -> x0, starting transfers between devices: 3.65 us -> none  [local(): lax.all_to_all(results, 'ep', split_axis=1, concat_axis=0, tiled=True)]
  transfers between devices with their start and end apart: 5 -> 0, of which waited for: 4 -> 0; matrix products, arithmetic and copies ran while one was open for 6% -> 0% of each run, Pallas kernels for 0% -> 0%
where the time goes in v1:
time: 66.7 us; the launch traced here: 66.4 us
  Pallas kernels  56.8 us (85%)
  local copies, waits for them, and re-layouts  8.99 us (13%)
    pallas_call x1, Pallas kernels, local(): pl.pallas_call(functools.partial(kernel, (ep, tp, zs, half, experts_here)...  56.8 us
    unnamed x5, local copies, waits for them, and re-layouts  8.99 us

profile of v1, /device:TPU:0, one launch (start us, length us, event | category | flops | bytes accessed | tf_op | source)
XLA Modules:
  0.0 66.4 jit_solution(425753265732943405)
XLA Ops:
  0.6 1.4 %copy.19.routes = s32[128,2]{1,0:T(8,128)} copy(s32[128,2]{0,1:T(2,128)} %param.26) | data formatting | bytes 2048 | tf_op args[11]
  2.0 2.2 %copy.17.router_group = bf16[4096,4]{1,0:T(8,128)(2,1)} copy(bf16[4096,4]{0,1:T(4,128)(2,1)} %param.24) | data formatting | bytes 65536 | tf_op args[9]
  4.2 2.3 %copy.18.router_expert = bf16[4096,16]{1,0:T(8,128)(2,1)} copy(bf16[4096,16]{0,1:T(8,128)(2,1)} %param.25) | data formatting | bytes 262144 | tf_op args[10]
  6.5 56.8 %mixer_and_experts.1 = (bf16[16,4096]{1,0:T(8,128)(2,1)}, bf16[16,4096]{1,0:T(8,128)(2,1)}) custom-call(bf16[128,4096]{1,0:T(8,128)(2,1)} %mix_tokens.1, f32[1,4096]{1,0:T(1,128)} %bitcast.2, bf16[4096,256]{1,0:T(8,128)(2,1)} %value_w.1, bf16[4096,256]{1,0:T(8,128)(2,1)} %inner_w.1, bf16[4096,256]{1,0:T(8,128)(2,1)} %outer_w.1, f32[3,256]{1,0:T(4,128)} %taps.1, ...), custom_call_target="tpu_custom_call" | custom-call | tf_op jit(solution)/shard_map/mixer_and_experts/pallas_call | solution.py:439
  63.2 1.6 %copy.22 = bf16[16,4096]{1,0:T(8,128)(2,1)} copy(bf16[16,4096]{1,0:T(8,128)(2,1)} %get-tuple-element.4) | data formatting | bytes 262144
  64.8 1.6 %copy.23 = bf16[16,4096]{1,0:T(8,128)(2,1)} copy(bf16[16,4096]{1,0:T(8,128)(2,1)} %get-tuple-element.5) | data formatting | bytes 262144

commit v2 on v1

--- a/solution.py
+++ b/solution.py
@@ -10,7 +10,8 @@
 EPG = 4
 CAP = 4
 CORES = 2
-CHUNKS = 4
+CHUNKS = 8
+PARTS = 4
 MESH = pl.DeviceIdType.MESH
 F32, BF16 = jnp.float32, jnp.bfloat16
 
@@ -46,9 +47,9 @@
     router_group, router_expert, routes, gate_w, up_w, down_w,
     mixer_out, expert_out,
     xm, xe, rg, rx, vw, iw, ow, mw, gw, uw, dw,
-    nm, ne, spread, pack, got, wpack, wgot, wrow,
-    gated, halo, padded, conv, pair_out, pair_in, keep, zin,
-    hid, y_out, y_in, y_keep, e_in, s_keep, s_out, s_in,
+    nm, ne, spread, gather, pack, got, wpack, wgot, wrow,
+    gated, halo, padded, conv, ordered, pair_out, pair_in, keep, zin,
+    gate_acc, up_acc, hid, both_y, y_out, y_in, y_keep, e_in, s_keep, s_out, s_in,
     load_sem, gate_sem, up_sem, down_sem,
     disp_s, disp_r, w_s, w_r, fwd_s, fwd_r, halo_s, halo_r, mp_s, mp_r, mz_s, mz_r,
     yp_s, yp_r, ye_s, ye_r, yz_s, yz_r,
@@ -92,13 +93,15 @@
             device_id={"ep": e, "tp": t}, device_id_type=MESH,
         )
 
-    loads[0].wait()
-    norm_rows(xe, moe_gain, ne)
     count = xe.shape[0]
     share = count // tp
     slots = half // zs
     span = ep * half
-    r = routes[...]
+    diagonal = jnp.where(iota((count, count), 0) == iota((count, count), 1), 1.0, 0.0)
+    r = lax.dot_general(
+        diagonal.astype(BF16), routes[...].astype(F32).astype(BF16), (((1,), (1,)), ((), ())),
+        preferred_element_type=F32,
+    ).astype(jnp.int32)
     picks = [r[:, 0:1], r[:, 1:2]]
     lane = iota((count, 128), 1)
     shards = [
@@ -117,14 +120,20 @@
         hits.append(slot_lane == base + s * half + mine)
     one_hot = jnp.where(hits[0] | hits[1], 1.0, 0.0).astype(BF16)
     spread[...] = one_hot
-
-    def pack_tile(cols):
-        pack[:, cols] = lax.dot_general(
-            spread[...], ne[:, cols], (((0,), (0,)), ((), ())), preferred_element_type=F32
+    gather[...] = lax.dot_general(
+        one_hot, diagonal.astype(BF16), (((0,), (0,)), ((), ())), preferred_element_type=F32
+    ).astype(BF16)
+    loads[0].wait()
+    norm_rows(xe, moe_gain, ne)
+    part = width // PARTS
+
+    def pack_part(q):
+        cols = slice(q * part, (q + 1) * part)
+        pack[:, cols] = jnp.dot(
+            gather[...], ne[:, cols], preferred_element_type=F32
         ).astype(BF16)
 
-    column_tiles(width, 512, pack_tile)
-
+    pack_part(0)
     pl.semaphore_wait(barrier, (ep - 1) + (zs - 1) + 1)
     sends = []
 
@@ -135,13 +144,21 @@
     def half_rows(c, e):
         return pl.ds(pl.multiple_of(c * span + e * half, half), half)
 
-    for e in ep_peers:
-        go(
-            remote(
-                pack.at[half_rows(c_me, e), :], got.at[half_rows(c_me, e_me), :],
-                disp_s.at[e], disp_r.at[e_me], e, t_me,
+    def dispatch(q):
+        cols = pl.ds(q * part, part)
+        for e in ep_peers:
+            go(
+                remote(
+                    pack.at[half_rows(c_me, e), cols], got.at[half_rows(c_me, e_me), cols],
+                    disp_s.at[q, e], disp_r.at[q, e_me], e, t_me,
+                )
             )
-        )
+
+    early = PARTS // 2
+    for q in range(1, PARTS):
+        if q <= early:
+            dispatch(q - 1)
+        pack_part(q)
     for k in range(experts_here):
         pltpu.make_async_copy(gate_w.at[k], gw.at[k], gate_sem.at[k]).start()
         pltpu.make_async_copy(up_w.at[k], uw.at[k], up_sem.at[k]).start()
@@ -150,8 +167,9 @@
 
     loads[1].wait()
     loads[2].wait()
-    group_exp = jnp.exp(jnp.dot(ne[...], rg[...], preferred_element_type=F32))
-    expert_logit = jnp.dot(ne[...], rx[...], preferred_element_type=F32)
+    lanes = (((1,), (1,)), ((), ()))
+    group_exp = jnp.exp(lax.dot_general(ne[...], rg[...], lanes, preferred_element_type=F32))
+    expert_logit = lax.dot_general(ne[...], rx[...], lanes, preferred_element_type=F32)
     groups, experts = group_exp.shape[1], expert_logit.shape[1]
     group = sum((picks[0] >= s * EPG).astype(jnp.int32) for s in range(1, groups))
     chosen_group = jnp.where(iota((count, groups), 1) == group, group_exp, 0.0)
@@ -171,17 +189,12 @@
     for _ in range(3):
         parts.append(rest.astype(BF16))
         rest = rest - parts[-1].astype(F32)
-    packed_w = sum(
-        lax.dot_general(spread[...], p, (((0,), (0,)), ((), ())), preferred_element_type=F32)
-        for p in parts
-    )
+    packed_w = sum(jnp.dot(gather[...], p, preferred_element_type=F32) for p in parts)
     for e in range(ep):
         for c in range(CORES):
             wpack[e, c * half : (c + 1) * half, :] = packed_w[
                 c * span + e * half : c * span + (e + 1) * half, :
             ]
-    for e in ep_peers:
-        go(remote(wpack.at[e], wgot.at[e_me], w_s.at[e], w_r.at[e_me], e, t_me))
     wgot[e_me] = wpack[e_me]
     for c in range(CORES):
         got[half_rows(c, e_me), :] = pack[half_rows(c, e_me), :]
@@ -199,6 +212,11 @@
         lax.rem(e_me + 1, ep), t_me,
     )
     halo_copy.start()
+    for q in range(early, PARTS):
+        dispatch(q)
+        if q == early:
+            for e in ep_peers:
+                go(remote(wpack.at[e], wgot.at[e_me], w_s.at[e], w_r.at[e_me], e, t_me))
     padded[8:, :] = gated[...].astype(F32)
     loads[6].wait()
     outer_proj = jnp.dot(nm[...], ow[...], preferred_element_type=F32)
@@ -224,21 +242,18 @@
     loads[7].wait()
     everything = slice(None)
 
-    def partner_tile(cols):
-        pair_out[:, cols] = jnp.dot(
-            parity_rows(conv, c_no, mix_share, everything), mw[:, cols], preferred_element_type=F32
-        ).astype(BF16)
-
-    column_tiles(width, 512, partner_tile)
+    mix_rows = zs * mix_share
+    ordered[0:mix_rows, :] = parity_rows(conv, c_no, mix_share, everything)
+    ordered[mix_rows:, :] = parity_rows(conv, c_me, mix_share, everything)
+
+    def mix_tile(cols):
+        both = jnp.dot(ordered[...], mw[:, cols], preferred_element_type=F32)
+        pair_out[:, cols] = both[0:mix_rows].astype(BF16)
+        keep[:, cols] = both[mix_rows:]
+
+    column_tiles(width, 512, mix_tile)
     pair_copy = remote(pair_out, pair_in, mp_s.at[0], mp_r.at[0], e_me, partner)
     go(pair_copy)
-
-    def own_tile(cols):
-        keep[:, cols] = jnp.dot(
-            parity_rows(conv, c_me, mix_share, everything), mw[:, cols], preferred_element_type=F32
-        )
-
-    column_tiles(width, 512, own_tile)
     pair_copy.wait_recv()
 
     def sum_tile(cols):
@@ -259,39 +274,60 @@
             )
         )
 
-    for e in ep_peers:
-        here = got.at[half_rows(c_me, e), :]
-        remote(here, here, disp_s.at[e], disp_r.at[e], e, t_me).wait_recv()
-        go(remote(here, here, fwd_s.at[e], fwd_r.at[e], e_me, partner))
-    for e in ep_peers:
-        remote(wgot.at[e], wgot.at[e], w_s.at[e], w_r.at[e], e, t_me).wait_recv()
-    for c in range(CORES):
-        for e in range(ep):
-            wrow[c * span + e * half : c * span + (e + 1) * half, :] = wgot[
-                e, c * half : (c + 1) * half, :
-            ]
-    for e in ep_peers:
-        there = got.at[half_rows(c_no, e), :]
-        remote(there, there, fwd_s.at[e], fwd_r.at[e], e_me, partner).wait_recv()
-
-    hidden = gw.shape[2]
+    def forward(q):
+        cols = pl.ds(q * part, part)
+        for e in ep_peers:
+            here = got.at[half_rows(c_me, e), cols]
+            remote(here, here, disp_s.at[q, e], disp_r.at[q, e], e, t_me).wait_recv()
+            go(remote(here, here, fwd_s.at[q, e], fwd_r.at[q, e], e_me, partner))
+
+    def forwarded(q):
+        cols = pl.ds(q * part, part)
+        for e in ep_peers:
+            there = got.at[half_rows(c_no, e), cols]
+            remote(there, there, fwd_s.at[q, e], fwd_r.at[q, e], e_me, partner).wait_recv()
+
     arrived_lane = iota((2 * span, 128), 1)
+
+    def project(q):
+        cols = slice(q * part, (q + 1) * part)
+
+        def expert(k, carry):
+            gate = jnp.dot(got[:, cols], gw[k, cols, :], preferred_element_type=F32)
+            up = jnp.dot(got[:, cols], uw[k, cols, :], preferred_element_type=F32)
+            if q:
+                gate = gate + gate_acc[k]
+                up = up + up_acc[k]
+            if q < PARTS - 1:
+                gate_acc[k] = gate
+                up_acc[k] = up
+                return carry
+            weight = jnp.sum(
+                jnp.where(arrived_lane == e_me * experts_here + k, wrow[...], 0.0),
+                axis=1, keepdims=True,
+            )
+            hid[k] = (gate / (1.0 + jnp.exp(-gate)) * up * weight).astype(BF16)
+            return carry
+
+        lax.fori_loop(0, experts_here, expert, 0)
+
+    forward(0)
     for k in range(experts_here):
         pltpu.make_async_copy(gate_w.at[k], gw.at[k], gate_sem.at[k]).wait()
         pltpu.make_async_copy(up_w.at[k], uw.at[k], up_sem.at[k]).wait()
-
-    def expert(k, carry):
-        gate = jnp.dot(got[...], gw[k], preferred_element_type=F32)
-        up = jnp.dot(got[...], uw[k], preferred_element_type=F32)
-        weight = jnp.sum(
-            jnp.where(arrived_lane == e_me * experts_here + k, wrow[...], 0.0),
-            axis=1, keepdims=True,
-        )
-        value = gate / (1.0 + jnp.exp(-gate)) * up * weight
-        hid[k] = value.astype(BF16)
-        return carry
-
-    lax.fori_loop(0, experts_here, expert, 0)
+    for q in range(PARTS):
+        if q + 1 < PARTS:
+            forward(q + 1)
+        else:
+            for e in ep_peers:
+                remote(wgot.at[e], wgot.at[e], w_s.at[e], w_r.at[e], e, t_me).wait_recv()
+            for c in range(CORES):
+                for e in range(ep):
+                    wrow[c * span + e * half : c * span + (e + 1) * half, :] = wgot[
+                        e, c * half : (c + 1) * half, :
+                    ]
+        forwarded(q)
+        project(q)
     for k in range(experts_here):
         pltpu.make_async_copy(down_w.at[k], dw.at[k], down_sem.at[k]).wait()
 
@@ -300,14 +336,6 @@
 
     def core_rows(c):
         return pl.ds(pl.multiple_of(c * span, span), span)
-
-    def down(c, cols):
-        total = jnp.dot(hid[0, core_rows(c), :], dw[0, :, cols], preferred_element_type=F32)
-        for k in range(1, experts_here):
-            total = total + jnp.dot(
-                hid[k, core_rows(c), :], dw[k, :, cols], preferred_element_type=F32
-            )
-        return total
 
     y_copies = {}
 
@@ -315,13 +343,14 @@
         for i in range(chunk // tile):
             at = slice(i * tile, (i + 1) * tile)
             cols = slice(j * chunk + i * tile, j * chunk + (i + 1) * tile)
-            y_out[j, :, at] = down(c_no, cols).astype(BF16)
+            both = jnp.dot(hid[0], dw[0, :, cols], preferred_element_type=F32)
+            for k in range(1, experts_here):
+                both = both + jnp.dot(hid[k], dw[k, :, cols], preferred_element_type=F32)
+            both_y[...] = both
+            y_out[j, :, at] = both_y[core_rows(c_no), :].astype(BF16)
+            y_keep[j % 2, :, at] = both_y[core_rows(c_me), :]
         y_copies[j] = remote(y_out.at[j], y_in.at[j], yp_s.at[j], yp_r.at[j], e_me, partner)
         go(y_copies[j])
-        for i in range(chunk // tile):
-            at = slice(i * tile, (i + 1) * tile)
-            cols = slice(j * chunk + i * tile, j * chunk + (i + 1) * tile)
-            y_keep[j % 2, :, at] = down(c_me, cols)
 
     def e_rows(e):
         return pl.ds(pl.multiple_of(e * half, half), half)
@@ -352,10 +381,10 @@
                     yz_s.at[j, z], yz_r.at[j, z_me], e_me, z * CORES + c_me,
                 )
             )
-        s_keep[j % 2] = total
+        s_keep[j % 4] = total
 
     def stage_d(j):
-        total = s_keep[j % 2, z_rows(z_me, share), :]
+        total = s_keep[j % 4, z_rows(z_me, share), :]
         for z in z_peers:
             here = s_in.at[j, z]
             remote(here, here, yz_s.at[j, z], yz_r.at[j, z], e_me, z * CORES + c_me).wait_recv()
@@ -375,11 +404,12 @@
         total = total + zin[z].astype(F32)
     mixer_out[...] = total.astype(BF16)
 
-    for j in range(CHUNKS):
-        stage_c(j)
-        if j:
-            stage_d(j - 1)
-    stage_d(CHUNKS - 1)
+    lag = 3
+    for j in range(CHUNKS + lag):
+        if j < CHUNKS:
+            stage_c(j)
+        if j >= lag:
+            stage_d(j - lag)
     for copy in sends:
         copy.wait_send()
 
@@ -406,26 +436,27 @@
     V, D = pltpu.VMEM, lambda *s: pltpu.SemaphoreType.DMA(s)
     scratch = [
         V((rows, width), BF16), V((count, width), BF16),
-        V(router_group.shape, BF16), V(router_expert.shape, BF16),
+        V(router_group.T.shape, BF16), V(router_expert.T.shape, BF16),
         V(value_w.shape, BF16), V(inner_w.shape, BF16), V(outer_w.shape, BF16),
         V(mix_w.shape, BF16),
         V(gate_w.shape, BF16), V(up_w.shape, BF16), V(down_w.shape, BF16),
-        V((rows, width), BF16), V((count, width), BF16), V((count, 2 * span), BF16),
+        V((rows, width), BF16), V((count, width), BF16), V((count, 2 * span), BF16), V((2 * span, count), BF16),
         V((2 * span, width), BF16), V((2 * span, width), BF16),
         V((ep, 2 * half, 128), F32), V((ep, 2 * half, 128), F32), V((2 * span, 128), F32),
         V((rows, channels), BF16), V((16, channels), BF16), V((rows + 8, channels), F32),
-        V((rows, channels), BF16),
+        V((rows, channels), BF16), V((rows, channels), BF16),
         V((zs * mix_share, width), BF16), V((zs * mix_share, width), BF16),
         V((zs * mix_share, width), F32),
         V((zs, mix_share, width), BF16),
-        V((experts_here, 2 * span, hidden), BF16),
+        V((experts_here, 2 * span, hidden), F32), V((experts_here, 2 * span, hidden), F32),
+        V((experts_here, 2 * span, hidden), BF16), V((2 * span, min(512, chunk)), F32),
         V((CHUNKS, span, chunk), BF16), V((CHUNKS, span, chunk), BF16),
         V((2, span, chunk), F32),
         V((CHUNKS, span, chunk), BF16),
-        V((2, zs * share, chunk), F32), V((CHUNKS, zs * share, chunk), BF16),
+        V((4, zs * share, chunk), F32), V((CHUNKS, zs * share, chunk), BF16),
         V((CHUNKS, zs, share, chunk), BF16),
         D(8), D(experts_here), D(experts_here), D(experts_here),
-        D(ep), D(ep), D(ep), D(ep), D(ep), D(ep), D(1), D(1), D(1), D(1), D(zs), D(zs),
+        D(PARTS, ep), D(PARTS, ep), D(ep), D(ep), D(PARTS, ep), D(PARTS, ep), D(1), D(1), D(1), D(1), D(zs), D(zs),
         D(CHUNKS), D(CHUNKS), D(CHUNKS, ep), D(CHUNKS, ep), D(CHUNKS, zs), D(CHUNKS, zs),
     ]
     out = [
@@ -448,7 +479,7 @@
         name="mixer_and_experts",
     )(
         mix_tokens, mix_gain.reshape(1, width), value_w, inner_w, outer_w, taps, mix_w,
-        moe_tokens, moe_gain.reshape(1, width), router_group, router_expert, routes,
+        moe_tokens, moe_gain.reshape(1, width), router_group.T, router_expert.T, routes.T,
         gate_w, up_w, down_w,
     )
 

time: 66.7 us -> 55.6 us (0.83)
  local copies, waits for them, and re-layouts: 8.99 us -> 3.14 us
  Pallas kernels: 56.8 us -> 51.6 us
    unnamed x5 -> x2, local copies, waits for them, and re-layouts: 8.99 us -> 3.14 us
    pallas_call x1, Pallas kernels: 56.8 us -> 51.6 us  [local(): pl.pallas_call(functools.partial(kernel, (ep, tp, zs, half, experts_here)...]
where the time goes in v2:
time: 55.6 us; the launch traced here: 55.4 us
  Pallas kernels  51.6 us (93%)
  local copies, waits for them, and re-layouts  3.14 us (6%)
  between operations  0.64 us (1%)
    pallas_call x1, Pallas kernels, local(): pl.pallas_call(functools.partial(kernel, (ep, tp, zs, half, experts_here)...  51.6 us
    unnamed x2, local copies, waits for them, and re-layouts  3.14 us

profile of v2, /device:TPU:0, one launch (start us, length us, event | category | flops | bytes accessed | tf_op | source)
XLA Modules:
  0.0 55.4 jit_solution(544535536933380706)
XLA Ops:
  0.6 51.6 %mixer_and_experts.1 = (bf16[16,4096]{1,0:T(8,128)(2,1)}, bf16[16,4096]{1,0:T(8,128)(2,1)}) custom-call(bf16[128,4096]{1,0:T(8,128)(2,1)} %mix_tokens.1, f32[1,4096]{1,0:T(1,128)} %bitcast.7, bf16[4096,256]{1,0:T(8,128)(2,1)} %value_w.1, bf16[4096,256]{1,0:T(8,128)(2,1)} %inner_w.1, bf16[4096,256]{1,0:T(8,128)(2,1)} %outer_w.1, f32[3,256]{1,0:T(4,128)} %taps.1, ...), custom_call_target="tpu_custom_call" | custom-call | tf_op jit(solution)/shard_map/mixer_and_experts/pallas_call | solution.py:470
  52.2 1.6 %copy.19 = bf16[16,4096]{1,0:T(8,128)(2,1)} copy(bf16[16,4096]{1,0:T(8,128)(2,1)} %get-tuple-element.4) | data formatting | bytes 262144
  53.8 1.6 %copy.20 = bf16[16,4096]{1,0:T(8,128)(2,1)} copy(bf16[16,4096]{1,0:T(8,128)(2,1)} %get-tuple-element.5) | data formatting | bytes 262144

commit v3 on v2

--- a/solution.py
+++ b/solution.py
@@ -11,7 +11,8 @@
 CAP = 4
 CORES = 2
 CHUNKS = 8
-PARTS = 4
+SPLIT = (2, 2, 3, 1)
+PARTS = len(SPLIT)
 MESH = pl.DeviceIdType.MESH
 F32, BF16 = jnp.float32, jnp.bfloat16
 
@@ -125,10 +126,14 @@
     ).astype(BF16)
     loads[0].wait()
     norm_rows(xe, moe_gain, ne)
-    part = width // PARTS
+    unit = width // sum(SPLIT)
+
+    def part_slice(q):
+        return sum(SPLIT[:q]) * unit, SPLIT[q] * unit
 
     def pack_part(q):
-        cols = slice(q * part, (q + 1) * part)
+        first, size = part_slice(q)
+        cols = slice(first, first + size)
         pack[:, cols] = jnp.dot(
             gather[...], ne[:, cols], preferred_element_type=F32
         ).astype(BF16)
@@ -145,7 +150,7 @@
         return pl.ds(pl.multiple_of(c * span + e * half, half), half)
 
     def dispatch(q):
-        cols = pl.ds(q * part, part)
+        cols = pl.ds(*part_slice(q))
         for e in ep_peers:
             go(
                 remote(
@@ -220,15 +225,10 @@
     padded[8:, :] = gated[...].astype(F32)
     loads[6].wait()
     outer_proj = jnp.dot(nm[...], ow[...], preferred_element_type=F32)
-    halo_copy.wait()
-    before = halo[...].astype(F32)[8:16, :]
-    padded[0:8, :] = jnp.where(e_me > 0, before, jnp.zeros_like(before))
-    n_taps = taps.shape[0]
-    mixed = taps[0:1, :] * padded[pl.ds(9 - n_taps, rows), :]
-    for j in range(1, n_taps):
-        mixed = mixed + taps[j : j + 1, :] * padded[pl.ds(9 - n_taps + j, rows), :]
-    conv[...] = (outer_proj * mixed).astype(BF16)
     mix_share = rows // tp
+    mix_rows = zs * mix_share
+    everything = slice(None)
+    pair_copy = remote(pair_out, pair_in, mp_s.at[0], mp_r.at[0], e_me, partner)
 
     def parity_rows(ref, c, step, cols):
         return jnp.concatenate(
@@ -239,50 +239,59 @@
             axis=0,
         )
 
-    loads[7].wait()
-    everything = slice(None)
-
-    mix_rows = zs * mix_share
-    ordered[0:mix_rows, :] = parity_rows(conv, c_no, mix_share, everything)
-    ordered[mix_rows:, :] = parity_rows(conv, c_me, mix_share, everything)
-
-    def mix_tile(cols):
-        both = jnp.dot(ordered[...], mw[:, cols], preferred_element_type=F32)
-        pair_out[:, cols] = both[0:mix_rows].astype(BF16)
-        keep[:, cols] = both[mix_rows:]
-
-    column_tiles(width, 512, mix_tile)
-    pair_copy = remote(pair_out, pair_in, mp_s.at[0], mp_r.at[0], e_me, partner)
-    go(pair_copy)
-    pair_copy.wait_recv()
-
-    def sum_tile(cols):
-        total = keep[:, cols] + pair_in[:, cols].astype(F32)
-        keep[:, cols] = total
-        pair_in[:, cols] = total.astype(BF16)
-
-    column_tiles(width, 512, sum_tile)
-
     def z_rows(z, step):
         return pl.ds(pl.multiple_of(z * step, step), step)
 
-    for z in z_peers:
-        go(
-            remote(
-                pair_in.at[z_rows(z, mix_share), :], zin.at[z_me], mz_s.at[z], mz_r.at[z_me],
-                e_me, z * CORES + c_me,
+    def mixer_pair():
+        halo_copy.wait()
+        before = halo[...].astype(F32)[8:16, :]
+        padded[0:8, :] = jnp.where(e_me > 0, before, jnp.zeros_like(before))
+        n_taps = taps.shape[0]
+        mixed = taps[0:1, :] * padded[pl.ds(9 - n_taps, rows), :]
+        for j in range(1, n_taps):
+            mixed = mixed + taps[j : j + 1, :] * padded[pl.ds(9 - n_taps + j, rows), :]
+        conv[...] = (outer_proj * mixed).astype(BF16)
+
+        loads[7].wait()
+
+        ordered[0:mix_rows, :] = parity_rows(conv, c_no, mix_share, everything)
+        ordered[mix_rows:, :] = parity_rows(conv, c_me, mix_share, everything)
+
+        def mix_tile(cols):
+            both = jnp.dot(ordered[...], mw[:, cols], preferred_element_type=F32)
+            pair_out[:, cols] = both[0:mix_rows].astype(BF16)
+            keep[:, cols] = both[mix_rows:]
+
+        column_tiles(width, 512, mix_tile)
+        go(pair_copy)
+
+    def mixer_sums():
+        pair_copy.wait_recv()
+
+        def sum_tile(cols):
+            total = keep[:, cols] + pair_in[:, cols].astype(F32)
+            keep[:, cols] = total
+            pair_in[:, cols] = total.astype(BF16)
+
+        column_tiles(width, 512, sum_tile)
+
+        for z in z_peers:
+            go(
+                remote(
+                    pair_in.at[z_rows(z, mix_share), :], zin.at[z_me], mz_s.at[z], mz_r.at[z_me],
+                    e_me, z * CORES + c_me,
+                )
             )
-        )
 
     def forward(q):
-        cols = pl.ds(q * part, part)
+        cols = pl.ds(*part_slice(q))
         for e in ep_peers:
             here = got.at[half_rows(c_me, e), cols]
             remote(here, here, disp_s.at[q, e], disp_r.at[q, e], e, t_me).wait_recv()
             go(remote(here, here, fwd_s.at[q, e], fwd_r.at[q, e], e_me, partner))
 
     def forwarded(q):
-        cols = pl.ds(q * part, part)
+        cols = pl.ds(*part_slice(q))
         for e in ep_peers:
             there = got.at[half_rows(c_no, e), cols]
             remote(there, there, fwd_s.at[q, e], fwd_r.at[q, e], e_me, partner).wait_recv()
@@ -290,7 +299,8 @@
     arrived_lane = iota((2 * span, 128), 1)
 
     def project(q):
-        cols = slice(q * part, (q + 1) * part)
+        first, size = part_slice(q)
+        cols = slice(first, first + size)
 
         def expert(k, carry):
             gate = jnp.dot(got[:, cols], gw[k, cols, :], preferred_element_type=F32)
@@ -318,6 +328,8 @@
     for q in range(PARTS):
         if q + 1 < PARTS:
             forward(q + 1)
+            if q == 1:
+                mixer_sums()
         else:
             for e in ep_peers:
                 remote(wgot.at[e], wgot.at[e], w_s.at[e], w_r.at[e], e, t_me).wait_recv()
@@ -328,6 +340,8 @@
                     ]
         forwarded(q)
         project(q)
+        if q == 0:
+            mixer_pair()
     for k in range(experts_here):
         pltpu.make_async_copy(down_w.at[k], dw.at[k], down_sem.at[k]).wait()
 
@@ -348,7 +362,7 @@
                 both = both + jnp.dot(hid[k], dw[k, :, cols], preferred_element_type=F32)
             both_y[...] = both
             y_out[j, :, at] = both_y[core_rows(c_no), :].astype(BF16)
-            y_keep[j % 2, :, at] = both_y[core_rows(c_me), :]
+            y_keep[j % 3, :, at] = both_y[core_rows(c_me), :]
         y_copies[j] = remote(y_out.at[j], y_in.at[j], yp_s.at[j], yp_r.at[j], e_me, partner)
         go(y_copies[j])
 
@@ -357,7 +371,7 @@
 
     def stage_b(j):
         y_copies[j].wait_recv()
-        y_in[j] = (y_keep[j % 2] + y_in[j].astype(F32)).astype(BF16)
+        y_in[j] = (y_keep[j % 3] + y_in[j].astype(F32)).astype(BF16)
         for e in ep_peers:
             go(
                 remote(
@@ -391,27 +405,37 @@
             total = total + s_in[j, z].astype(F32)
         expert_out[:, j * chunk : (j + 1) * chunk] = total.astype(BF16)
 
-    for j in range(CHUNKS):
-        stage_a(j)
-        if j:
-            stage_b(j - 1)
-    stage_b(CHUNKS - 1)
-
-    total = keep[z_rows(z_me, mix_share), :]
-    for z in z_peers:
-        here = zin.at[z]
-        remote(here, here, mz_s.at[z], mz_r.at[z], e_me, z * CORES + c_me).wait_recv()
-        total = total + zin[z].astype(F32)
-    mixer_out[...] = total.astype(BF16)
-
-    lag = 3
-    for j in range(CHUNKS + lag):
-        if j < CHUNKS:
-            stage_c(j)
-        if j >= lag:
-            stage_d(j - lag)
+    def mixer_final():
+        total = keep[z_rows(z_me, mix_share), :]
+        for z in z_peers:
+            here = zin.at[z]
+            remote(here, here, mz_s.at[z], mz_r.at[z], e_me, z * CORES + c_me).wait_recv()
+            total = total + zin[z].astype(F32)
+        mixer_out[...] = total.astype(BF16)
+
+    lag_b, lag_c, lag_d = 2, 7, 10
+    for step in range(CHUNKS + lag_d):
+        for stage, lag in ((stage_a, 0), (stage_b, lag_b), (stage_c, lag_c), (stage_d, lag_d)):
+            if 0 <= step - lag < CHUNKS:
+                stage(step - lag)
+        if step == CHUNKS:
+            mixer_final()
+
     for copy in sends:
         copy.wait_send()
+
+
+def store(a, b, a_out, b_out, held, sem):
+    refs = ((a, a_out), (b, b_out))
+    into = [pltpu.make_async_copy(s, held.at[i], sem.at[0, i]) for i, (s, _) in enumerate(refs)]
+    outof = [pltpu.make_async_copy(held.at[i], d, sem.at[1, i]) for i, (_, d) in enumerate(refs)]
+    for c in into:
+        c.start()
+    for c, d in zip(into, outof):
+        c.wait()
+        d.start()
+    for d in outof:
+        d.wait()
 
 
 def local(ep, tp, *args):
@@ -451,7 +475,7 @@
         V((experts_here, 2 * span, hidden), F32), V((experts_here, 2 * span, hidden), F32),
         V((experts_here, 2 * span, hidden), BF16), V((2 * span, min(512, chunk)), F32),
         V((CHUNKS, span, chunk), BF16), V((CHUNKS, span, chunk), BF16),
-        V((2, span, chunk), F32),
+        V((3, span, chunk), F32),
         V((CHUNKS, span, chunk), BF16),
         V((4, zs * share, chunk), F32), V((CHUNKS, zs * share, chunk), BF16),
         V((CHUNKS, zs, share, chunk), BF16),
@@ -467,7 +491,7 @@
         any_ref, vmem, any_ref, any_ref, any_ref, vmem, any_ref, any_ref, vmem,
         any_ref, any_ref, vmem, any_ref, any_ref, any_ref,
     ]
-    return pl.pallas_call(
+    results = pl.pallas_call(
         functools.partial(kernel, (ep, tp, zs, half, experts_here)),
         out_shape=out,
         in_specs=in_specs,
@@ -482,6 +506,14 @@
         moe_tokens, moe_gain.reshape(1, width), router_group.T, router_expert.T, routes.T,
         gate_w, up_w, down_w,
     )
+    return pl.pallas_call(
+        store,
+        out_shape=out,
+        in_specs=[any_ref, any_ref],
+        out_specs=[any_ref, any_ref],
+        scratch_shapes=[V((2, share, width), BF16), D(2, 2)],
+        name="store",
+    )(*results)
 
 
 def solution(mesh):

time: 55.6 us -> 50.9 us (0.915)
  local copies, waits for them, and re-layouts: 3.14 us -> 0 us
  Pallas kernels: 51.6 us -> 50.1 us
    pallas_call x1, Pallas kernels: 51.6 us -> 48.4 us  [local(): pl.pallas_call(functools.partial(kernel, (ep, tp, zs, half, experts_here)...]
    unnamed x2 -> x0, local copies, waits for them, and re-layouts: 3.14 us -> none
    pallas_call x0 -> x1, Pallas kernels: none -> 1.66 us  [local(): pl.pallas_call(store, out_shape=out, in_specs=[any_ref, any_ref], out_spe...]
where the time goes in v3:
time: 50.9 us; the launch traced here: 50.7 us
  Pallas kernels  50.1 us (98%)
  between operations  0.64 us (1%)
    pallas_call x1, Pallas kernels, local(): pl.pallas_call(functools.partial(kernel, (ep, tp, zs, half, experts_here)...  48.4 us
    pallas_call x1, Pallas kernels, local(): pl.pallas_call(store, out_shape=out, in_specs=[any_ref, any_ref], out_spe...  1.66 us

profile of v3, /device:TPU:0, one launch (start us, length us, event | category | flops | bytes accessed | tf_op | source)
XLA Modules:
  0.0 50.7 jit_solution(84259980728872417)
XLA Ops:
  0.6 48.4 %mixer_and_experts.1 = (bf16[16,4096]{1,0:T(8,128)(2,1)}, bf16[16,4096]{1,0:T(8,128)(2,1)}) custom-call(bf16[128,4096]{1,0:T(8,128)(2,1)} %mix_tokens.1, f32[1,4096]{1,0:T(1,128)} %bitcast.7, bf16[4096,256]{1,0:T(8,128)(2,1)} %value_w.1, bf16[4096,256]{1,0:T(8,128)(2,1)} %inner_w.1, bf16[4096,256]{1,0:T(8,128)(2,1)} %outer_w.1, f32[3,256]{1,0:T(4,128)} %taps.1, ...), custom_call_target="tpu_custom_call" | custom-call | tf_op jit(solution)/shard_map/mixer_and_experts/pallas_call | solution.py:494
  49.1 1.7 %store.1 = (bf16[16,4096]{1,0:T(8,128)(2,1)}, bf16[16,4096]{1,0:T(8,128)(2,1)}) custom-call(bf16[16,4096]{1,0:T(8,128)(2,1)} %get-tuple-element.4.a, bf16[16,4096]{1,0:T(8,128)(2,1)} %get-tuple-element.5.b), custom_call_target="tpu_custom_call" | custom-call | tf_op jit(solution)/shard_map/store/pallas_call | solution.py:509

commit v4 on v3

--- a/solution.py
+++ b/solution.py
@@ -125,6 +125,11 @@
         one_hot, diagonal.astype(BF16), (((0,), (0,)), ((), ())), preferred_element_type=F32
     ).astype(BF16)
     loads[0].wait()
+    for k in range(experts_here):
+        pltpu.make_async_copy(gate_w.at[k], gw.at[k], gate_sem.at[k]).start()
+        pltpu.make_async_copy(up_w.at[k], uw.at[k], up_sem.at[k]).start()
+    for k in range(experts_here):
+        pltpu.make_async_copy(down_w.at[k], dw.at[k], down_sem.at[k]).start()
     norm_rows(xe, moe_gain, ne)
     unit = width // sum(SPLIT)
 
@@ -164,12 +169,6 @@
         if q <= early:
             dispatch(q - 1)
         pack_part(q)
-    for k in range(experts_here):
-        pltpu.make_async_copy(gate_w.at[k], gw.at[k], gate_sem.at[k]).start()
-        pltpu.make_async_copy(up_w.at[k], uw.at[k], up_sem.at[k]).start()
-    for k in range(experts_here):
-        pltpu.make_async_copy(down_w.at[k], dw.at[k], down_sem.at[k]).start()
-
     loads[1].wait()
     loads[2].wait()
     lanes = (((1,), (1,)), ((), ()))

time: 50.9 us -> 50.8 us (level)
  no operation moved by 1% of the time
where the time goes in v4:
time: 50.8 us; the launch traced here: 50.6 us
  Pallas kernels  50 us (98%)
  between operations  0.64 us (1%)
    pallas_call x1, Pallas kernels, local(): pl.pallas_call(functools.partial(kernel, (ep, tp, zs, half, experts_here)...  48.3 us
    pallas_call x1, Pallas kernels, local(): pl.pallas_call(store, out_shape=out, in_specs=[any_ref, any_ref], out_spe...  1.66 us

profile of v4, /device:TPU:0, one launch (start us, length us, event | category | flops | bytes accessed | tf_op | source)
XLA Modules:
  0.0 50.6 jit_solution(14560396808444789388)
XLA Ops:
  0.6 48.3 %mixer_and_experts.1 = (bf16[16,4096]{1,0:T(8,128)(2,1)}, bf16[16,4096]{1,0:T(8,128)(2,1)}) custom-call(bf16[128,4096]{1,0:T(8,128)(2,1)} %mix_tokens.1, f32[1,4096]{1,0:T(1,128)} %bitcast.7, bf16[4096,256]{1,0:T(8,128)(2,1)} %value_w.1, bf16[4096,256]{1,0:T(8,128)(2,1)} %inner_w.1, bf16[4096,256]{1,0:T(8,128)(2,1)} %outer_w.1, f32[3,256]{1,0:T(4,128)} %taps.1, ...), custom_call_target="tpu_custom_call" | custom-call | tf_op jit(solution)/shard_map/mixer_and_experts/pallas_call | solution.py:493
  49.0 1.7 %store.1 = (bf16[16,4096]{1,0:T(8,128)(2,1)}, bf16[16,4096]{1,0:T(8,128)(2,1)}) custom-call(bf16[16,4096]{1,0:T(8,128)(2,1)} %get-tuple-element.4.a, bf16[16,4096]{1,0:T(8,128)(2,1)} %get-tuple-element.5.b), custom_call_target="tpu_custom_call" | custom-call | tf_op jit(solution)/shard_map/store/pallas_call | solution.py:508
